TPU v7x, 32 devices: a whole 2x2x4 slice. The times are simulated.
32 devices in a mesh: sp: 8 (over z, x), tp: 4 (over y, core).
Axes of the slice: x: 2, y: 2, z: 4, core: 2. Of those that a mesh axis runs over, the one named last changes fastest.
Arguments:
- wide_query: bfloat16 [4096, 1536], P('sp', 'tp'), may hold values from -6 to 6
- wide_key: bfloat16 [4096, 1536], P('sp', 'tp'), may hold values from -6 to 6
- wide_value: bfloat16 [4096, 1536], P('sp', 'tp'), may hold values from -6 to 6
- wide_gate: bfloat16 [4096, 1536], P('sp', 'tp'), may hold values from -6 to 6
- narrow_query: bfloat16 [4096, 512], P('sp', 'tp'), may hold values from -6 to 6
- narrow_key: bfloat16 [4096, 512], P('sp', 'tp'), may hold values from -6 to 6
- narrow_value: bfloat16 [4096, 512], P('sp', 'tp'), may hold values from -6 to 6
- narrow_gate: bfloat16 [4096, 512], P('sp', 'tp'), may hold values from -6 to 6
- wide_decay: float32 [12, 4096], P('tp', 'sp'), may hold values from -1 to 0
- narrow_decay: float32 [8, 4096], P('tp', 'sp'), may hold values from -1 to 0
- residual: bfloat16 [4096, 2048], P(('sp', 'tp')), may hold values from -6 to 6
- wide_out: bfloat16 [1536, 2048], P('tp'), may hold values from -0.125 to 0.125
- narrow_out: bfloat16 [512, 2048], P('tp'), may hold values from -0.125 to 0.125
- up_weight: bfloat16 [2048, 8192], P('sp', 'tp'), may hold values from -0.125 to 0.125
- down_weight: bfloat16 [8192, 2048], P('tp', 'sp'), may hold values from -0.0625 to 0.0625
- gain_mix: float32 [2048], replicated, may hold values from 0.1 to 1.9
- gain_pre: float32 [2048], replicated, may hold values from 0.1 to 1.9
- gain_mlp: float32 [2048], replicated, may hold values from 0.1 to 1.9
Outputs:
- result: bfloat16 [4096, 2048], P(('sp', 'tp'))
All inputs are finite; a program needn't handle non-finite values.
Results may differ from a plain program's by a relative error of at most 0.02.
Values may be sent and summed in bfloat16 or wider, within the bound.
A program may use at most 128 MiB of HBM per device.

v0:
```python
import jax
import jax.numpy as jnp
from jax import lax
from jax.sharding import PartitionSpec as P

WIDE_DIM = 128
NARROW_DIM = 64
SPAN = 128
epsilon = 1e-06


def prefix_2(array, axis, join, neutral):
    place = lax.axis_index(axis)
    gathered = jax.tree.map(
        lambda a, kind: lax.all_gather(a.astype(kind), axis),
        array,
        (jnp.bfloat16, jnp.bfloat16, jnp.bfloat16, jnp.bfloat16),
    )
    state = jax.tree.map(lambda a, e: jnp.zeros_like(a) + jnp.asarray(e, a.dtype), array, neutral)

    def one(turn, state):
        return join(
            state,
            jax.tree.map(
                lambda a, own: lax.dynamic_index_in_dim(a, turn, 0, False).astype(own.dtype),
                gathered,
                array,
            ),
        )

    return lax.fori_loop(0, place, one, state)


def rotate(packed, head_dim, positions):
    length = packed.shape[0]
    grouped = packed.astype(jnp.float32).reshape(length, -1, head_dim)
    halfway = head_dim // 2
    inverse = 10000.0 ** (-jnp.arange(0, head_dim, 2, dtype=jnp.float32) / head_dim)
    angles = positions.astype(jnp.float32)[:, None] * inverse[None, :]
    cosine_table = jnp.cos(angles)[:, None, :]
    sine_table = jnp.sin(angles)[:, None, :]
    leading = grouped[..., :halfway]
    trailing = grouped[..., halfway:]
    return jnp.concatenate(
        [
            leading * cosine_table - trailing * sine_table,
            leading * sine_table + trailing * cosine_table,
        ],
        axis=-1,
    )


def rms_scale(values, gain_vector):
    return (
        values
        * lax.rsqrt(jnp.mean(values * values, axis=-1, keepdims=True) + epsilon)
        * gain_vector
    )


def span_terms(query, key, value, log_decay, head_dim, offset):
    length = query.shape[0]
    count_of_heads = query.shape[1] // head_dim
    span_count = length // SPAN
    shaped = (span_count, SPAN, count_of_heads, head_dim)
    positions = offset + jnp.arange(length, dtype=jnp.int32)
    queries = rotate(query, head_dim, positions).astype(jnp.bfloat16).reshape(shaped)
    keys_full = (rotate(key, head_dim, positions) * head_dim ** (-0.5)).reshape(shaped)
    keys_half = keys_full.astype(jnp.bfloat16)
    values_all = value.reshape(shaped)
    cumulative = jnp.cumsum(log_decay.T.reshape(span_count, SPAN, count_of_heads), axis=1)
    causal = jnp.arange(SPAN)[:, None] >= jnp.arange(SPAN)[None, :]
    scores = jnp.einsum("nihd,njhd->nhij", queries, keys_half, preferred_element_type=jnp.float32)
    decay_rows = cumulative.transpose(0, 2, 1)
    log_gaps = jnp.where(causal, decay_rows[..., :, None] - decay_rows[..., None, :], -jnp.inf)
    weights = (scores * jnp.exp(log_gaps)).astype(jnp.bfloat16)
    within = jnp.einsum("nhij,njhd->nihd", weights, values_all, preferred_element_type=jnp.float32)
    span_total = cumulative[:, -1, :]
    scaled = (keys_full * jnp.exp(span_total[:, None, :] - cumulative)[..., None]).astype(
        jnp.bfloat16
    )
    own_state = jnp.einsum(
        "njhd,njhe->nhde", scaled, values_all, preferred_element_type=jnp.float32
    )

    def advance(carried, inputs):
        decay_sum, contribution = inputs
        return (carried * jnp.exp(decay_sum)[:, None, None] + contribution, carried)

    initial = jnp.zeros((count_of_heads, head_dim, head_dim), jnp.float32)
    closing, before = lax.scan(advance, initial, (span_total, own_state))
    device_decay = jnp.exp(jnp.sum(span_total, axis=0))
    return (queries, cumulative, within, span_total, before, closing, device_decay)


def finish(parts, prefix, gate, head_dim):
    queries, cumulative, within, span_total, before, closing, device_decay = parts
    length = gate.shape[0]
    earlier = jnp.cumsum(span_total, axis=0) - span_total
    entering = (prefix[None] * jnp.exp(earlier)[:, :, None, None] + before).astype(jnp.bfloat16)
    across = (
        jnp.einsum("nihd,nhde->nihe", queries, entering, preferred_element_type=jnp.float32)
        * jnp.exp(cumulative)[..., None]
    )
    output = (within + across).reshape(length, -1, head_dim)
    normed = output * lax.rsqrt(jnp.mean(output * output, axis=-1, keepdims=True) + epsilon)
    return (normed.reshape(length, -1) * jax.nn.silu(gate.astype(jnp.float32))).astype(jnp.bfloat16)


def combine_states(former, latter):
    return (
        former[0] * latter[0],
        former[1] * latter[0][:, None, None] + latter[1],
        former[2] * latter[2],
        former[3] * latter[2][:, None, None] + latter[3],
    )


def local(
    wide_query,
    wide_key,
    wide_value,
    wide_gate,
    narrow_query,
    narrow_key,
    narrow_value,
    narrow_gate,
    wide_decay,
    narrow_decay,
    residual,
    wide_out,
    narrow_out,
    up_weight,
    down_weight,
    gain_mix,
    gain_pre,
    gain_mlp,
):
    length = wide_query.shape[0]
    offset = lax.axis_index("sp") * length
    wide_parts = span_terms(wide_query, wide_key, wide_value, wide_decay, WIDE_DIM, offset)
    narrow_parts = span_terms(
        narrow_query, narrow_key, narrow_value, narrow_decay, NARROW_DIM, offset
    )
    identity = (
        jnp.ones_like(wide_parts[6]),
        jnp.zeros_like(wide_parts[5]),
        jnp.ones_like(narrow_parts[6]),
        jnp.zeros_like(narrow_parts[5]),
    )
    prefixes = prefix_2(
        (wide_parts[6], wide_parts[5], narrow_parts[6], narrow_parts[5]),
        "sp",
        combine_states,
        identity,
    )
    wide_mixed = finish(wide_parts, prefixes[1], wide_gate, WIDE_DIM)
    narrow_mixed = finish(narrow_parts, prefixes[3], narrow_gate, NARROW_DIM)
    wide_rows, narrow_rows = (
        lax.all_to_all(wide_mixed, "tp", split_axis=0, concat_axis=1, tiled=True),
        lax.all_to_all(narrow_mixed, "tp", split_axis=0, concat_axis=1, tiled=True),
    )
    wide_whole, narrow_whole = (
        lax.all_gather(wide_out, "tp", axis=0, tiled=True),
        lax.all_gather(narrow_out, "tp", axis=0, tiled=True),
    )
    projected = jnp.dot(wide_rows, wide_whole, preferred_element_type=jnp.float32) + jnp.dot(
        narrow_rows, narrow_whole, preferred_element_type=jnp.float32
    )
    updated = (residual.astype(jnp.float32) + rms_scale(projected, gain_mix)).astype(jnp.bfloat16)
    normed = rms_scale(updated.astype(jnp.float32), gain_pre).astype(jnp.bfloat16)
    block_rows = lax.all_gather(normed, "tp", axis=0, tiled=True)
    rectified = jax.nn.relu(
        jnp.dot(
            block_rows,
            lax.all_gather(up_weight, "sp", axis=0, tiled=True),
            preferred_element_type=jnp.float32,
        )
    )
    hidden = (rectified * rectified).astype(jnp.bfloat16)
    partial_terms = jnp.dot(
        hidden,
        lax.all_gather(down_weight, "sp", axis=1, tiled=True),
        preferred_element_type=jnp.float32,
    )
    lowered = lax.psum_scatter(
        partial_terms.astype(jnp.bfloat16), "tp", scatter_dimension=0, tiled=True
    ).astype(jnp.float32)
    return (updated.astype(jnp.float32) + rms_scale(lowered, gain_mlp)).astype(jnp.bfloat16)


def solution(mesh):
    return jax.shard_map(
        local,
        mesh=mesh,
        in_specs=(
            P("sp", "tp"),
            P("sp", "tp"),
            P("sp", "tp"),
            P("sp", "tp"),
            P("sp", "tp"),
            P("sp", "tp"),
            P("sp", "tp"),
            P("sp", "tp"),
            P("tp", "sp"),
            P("tp", "sp"),
            P(("sp", "tp"), None),
            P("tp", None),
            P("tp", None),
            P("sp", "tp"),
            P("tp", "sp"),
            P(),
            P(),
            P(),
        ),
        out_specs=P(("sp", "tp"), None),
        check_vma=False,
    )
```

profile of v0, /device:TPU:0, one launch (start us, length us, event | category | flops | bytes accessed | tf_op | source)
XLA Modules:
  0.0 507.7 jit_solution(15633803309684791243)
XLA Ops:
  8.1 1.2 copy.77
  10.2 1.0 subtract_convert_fusion
  14.4 3.3 while.42
  17.7 33.8 %all-gather.1 = bf16[24,128,128]{2,1,0:T(8,128)(2,1)S(1)} all-gather(bf16[3,128,128]{2,1,0:T(8,128)(2,1)S(1)} %convert_element_type.154), channel_id=3, replica_groups=mesh['sp'=8,'tp'=4] {'sp'}, dimensions={0}, use_global_device_ids=true | all-gather | bytes 884736 | tf_op jit(solution)/shard_map/all_gather | solution.py:15
  51.6 1.0 multiply_cosine_fusion.1
  52.5 1.7 copy.93
  54.2 0.9 convert.30
  55.1 1.7 copy.106
  56.8 0.9 convert.31
  57.8 1.6 fusion.61
  60.1 0.9 copy.122
  61.0 1.2 reduce_window_sum.45
  63.0 0.9 fusion.74
  63.9 1.1 copy.97
  65.0 1.8 reshape.384
  66.7 1.7 copy.99
  68.5 1.6 bitcast_dynamic-update-slice_fusion.2
  70.0 1.9 fusion.54
  71.9 6.2 %while.43 = (s32[]{:T(128)}, f32[2,64,64]{2,1,0:T(8,128)S(1)}, f32[4,2,64,64]{3,2,1,0:T(8,128)}, f32[4,2]{1,0:T(4,128)S(1)}, f32[4,2,64,64]{3,2,1,0:T(8,128)}, /*index=5*/s32[]{:T(128)}, s32[]{:T(128)}) while((s32[]{:T(128)}, f32[2,64,64]{2,1,0:T(8,128)S(1)}, f32[4,2,64,64]{3,2,1,0:T(8,128)}, f32[4,2]{1,0:T(4,128)S(1)}, ...), condition=%wide.region_7.8_spmd.clone, body=%wide.region_6.7_spmd.clone.sunk | while | flops 32771 | bytes 197240 | solution.py:91
  72.5 0.9 bitcast_add_fusion.5
  74.1 0.9 bitcast_add_fusion.5
  75.7 0.9 bitcast_add_fusion.5
  77.2 0.9 bitcast_add_fusion.5
  78.1 32.7 %all-gather.3 = bf16[16,64,64]{2,1,0:T(8,128)(2,1)} all-gather(bf16[2,64,64]{2,1,0:T(8,128)(2,1)S(1)} %convert_element_type.158), channel_id=5, replica_groups=mesh['sp'=8,'tp'=4] {'sp'}, dimensions={0}, use_global_device_ids=true | all-gather | bytes 147456 | tf_op jit(solution)/shard_map/all_gather | solution.py:15
  111.6 1.3 dynamic-slice
  114.6 21.4 %all-reduce.2 = (bf16[24]{0:T(256)(128)(2,1)S(1)}, bf16[16]{0:T(256)(128)(2,1)S(1)}) all-reduce(bf16[24]{0:T(256)(128)(2,1)S(1)} %dynamic-update-slice, bf16[16]{0:T(256)(128)(2,1)S(1)} %dynamic-update-slice.1), channel_id=2, replica_groups=mesh['sp'=8,'tp'=4] {'sp'}, use_global_device_ids=true, to_apply=%add | all-reduce | flops 40 | bytes 160
  136.2 1.0 concatenate.34
  137.5 1.7 concatenate.35
  139.1 1.2 copy.79
  140.3 1.1 copy.102
  142.1 2.6 fusion.8
  144.7 3.1 multiply_reduce_fusion.1
  147.8 1.7 copy.103
  149.6 1.2 copy.104
  151.0 0.8 copy_bitcast_fusion
  151.8 3.5 all-to-all-start
  157.8 4.8 all-to-all-done
  162.7 3.3 all-to-all-start.1
  166.3 3.8 fusion.77
  170.6 2.1 multiply_reduce_fusion
  173.1 1.0 fusion.20
  175.4 24.6 %all-gather.14.cloned.1.call-done = bf16[512,2048]{1,0:T(8,128)(2,1)} async-done(((bf16[128,2048]{1,0:T(8,128)(2,1)}), bf16[512,2048]{1,0:T(8,128)(2,1)}) %all-gather.14.cloned.1.call-update) | async-done | bytes 2097168 | tf_op jit(solution)/shard_map/all_gather | solution.py:172
  200.0 126.5 %all-gather.16.cloned.1.call-done = bf16[2048,2048]{1,0:T(8,128)(2,1)} async-done(((bf16[256,2048]{1,0:T(8,128)(2,1)}), bf16[2048,2048]{1,0:T(8,128)(2,1)}) %all-gather.16.cloned.1.call-update) | async-done | bytes 8388624 | tf_op jit(solution)/shard_map/all_gather | solution.py:176
  326.4 125.0 %all-gather.18.cloned.1.call-done = bf16[2048,2048]{1,0:T(8,128)(2,1)} async-done(((bf16[2048,256]{1,0:T(8,128)(2,1)}), bf16[2048,2048]{1,0:T(8,128)(2,1)}) %all-gather.18.cloned.1.call-update) | async-done | bytes 8388624 | tf_op jit(solution)/shard_map/all_gather | solution.py:183
  451.5 16.5 %convolution_convert_fusion = bf16[512,2048]{1,0:T(8,128)(2,1)} fusion(bf16[2048,2048]{1,0:T(8,128)(2,1)} %all-gather.18.cloned.1.call-done, bf16[512,2048]{1,0:T(8,128)(2,1)} %all-gather.14.cloned.1.call-done, bf16[2048,2048]{1,0:T(8,128)(2,1)} %all-gather.16.cloned.1.call-done), kind=kOutput, calls=%fused_computation.19 | convolution fusion | flops 8594128896 | bytes 20971520 | tf_op jit(solution)/shard_map/dot_general | solution.py:181
  468.0 29.5 %reduce-scatter.2.cloned.1.call-done = bf16[128,2048]{1,0:T(8,128)(2,1)} async-done(((bf16[512,2048]{1,0:T(8,128)(2,1)}), bf16[128,2048]{1,0:T(8,128)(2,1)}) %reduce-scatter.2.cloned.1.call-update) | async-done | bytes 524304 | tf_op jit(solution)/shard_map/reduce_scatter | solution.py:186
  497.5 1.2 fusion.16
  498.8 2.1 fusion.21
  (137 shorter events, 20.3 us)
Async XLA Ops:
  6.5 2.8 copy-start.7
  6.5 159.7 %all-gather.10.cloned.1.call-start = ((), (), s32[]{:S(2)}) async-start(), calls=%async_computation.3 | async-start | bytes 7864320 | tf_op jit(solution)/shard_map/all_gather | solution.py:164
  7.3 163.3 %all-gather.12.cloned.1.call-start = ((), (), s32[]{:S(2)}) async-start(), calls=%async_computation.4 | async-start | bytes 2621440 | tf_op jit(solution)/shard_map/all_gather | solution.py:165
  9.6 2.5 copy-start.17
  10.2 3.2 copy-start.6
  14.4 45.7 %copy-start.18 = (f32[2,512]{1,0:T(2,128)S(1)}, f32[2,512]{1,0:T(2,128)}, u32[]{:S(2)}) copy-start(f32[2,512]{1,0:T(2,128)} %param.33) | copy-start | bytes 12292
  62.2 74.0 %copy-start = (f32[4,128,2]{2,1,0:T(8,128)}, f32[4,128,2]{2,1,0:T(8,128)S(1)}, u32[]{:S(2)}) copy-start(f32[4,128,2]{2,1,0:T(8,128)S(1)} %reduce_window_sum.45) | copy-start | bytes 12292
  62.9 1.0 copy-start.12
  144.7 11.0 %copy-start.1 = (f32[4,128,2]{2,1,0:T(8,128)S(1)}, f32[4,128,2]{2,1,0:T(8,128)}, u32[]{:S(2)}) copy-start(f32[4,128,2]{2,1,0:T(8,128)} %copy-done) | copy-start | bytes 12292
  144.7 11.1 %copy-start.8 = (bf16[2,4,4,8,128]{4,3,2,1,0:T(8,128)(2,1)S(1)}, bf16[2,4,4,8,128]{4,3,2,1,0:T(8,128)(2,1)}, u32[]{:S(2)}) copy-start(bf16[2,4,4,8,128]{4,3,2,1,0:T(8,128)(2,1)} %get-tuple-element.233) | copy-start | bytes 196612
  147.8 7.5 %copy-start.13 = (f32[4,1,2]{0,2,1:T(2,128)S(1)}, f32[4,1,2]{0,2,1:T(2,128)}, u32[]{:S(2)}) copy-start(f32[4,1,2]{0,2,1:T(2,128)} %copy-done.12) | copy-start | bytes 100
  147.8 7.7 %copy-start.2 = (f32[4,128,2]{2,1,0:T(8,128)S(1)}, f32[4,128,2]{2,1,0:T(8,128)}, u32[]{:S(2)}) copy-start(f32[4,128,2]{2,1,0:T(8,128)} %get-tuple-element.236) | copy-start | bytes 12292
  147.8 8.1 %copy-start.9 = (f32[4,2,64,64]{3,2,1,0:T(8,128)S(1)}, f32[4,2,64,64]{3,2,1,0:T(8,128)}, u32[]{:S(2)}) copy-start(f32[4,2,64,64]{3,2,1,0:T(8,128)} %get-tuple-element.136) | copy-start | bytes 393220
  147.8 8.4 %copy-start.3 = (f32[4,128,2,64]{1,3,2,0:T(8,128)S(1)}, f32[4,128,2,64]{1,3,2,0:T(8,128)}, u32[]{:S(2)}) copy-start(f32[4,128,2,64]{1,3,2,0:T(8,128)} %bitcast_dynamic-update-slice_fusion.2) | copy-start | bytes 786436
  147.8 8.4 %copy-start.4 = (bf16[4,128,2,64]{1,3,2,0:T(8,128)(2,1)S(1)}, bf16[4,128,2,64]{1,3,2,0:T(8,128)(2,1)}, u32[]{:S(2)}) copy-start(bf16[4,128,2,64]{1,3,2,0:T(8,128)(2,1)} %copy.99) | copy-start | bytes 393220
  147.8 8.4 %copy-start.11 = (pred[128,128]{1,0:T(8,128)(4,1)S(1)}, pred[128,128]{1,0:T(8,128)(4,1)}, u32[]{:S(2)}) copy-start(pred[128,128]{1,0:T(8,128)(4,1)} %iota_compare_fusion) | copy-start | bytes 49156
  147.8 9.1 %copy-start.10 = (bf16[512,128]{1,0:T(8,128)(2,1)S(1)}, bf16[512,128]{1,0:T(8,128)(2,1)}, u32[]{:S(2)}) copy-start(bf16[512,128]{1,0:T(8,128)(2,1)} %param.31) | copy-start | bytes 393220
  151.8 10.8 %all-to-all-start = ((bf16[4,128,384]{1,2,0:T(8,128)(2,1)}), bf16[4,128,384]{1,2,0:T(8,128)(2,1)S(1)}, u32[]{:S(2)}, u32[]{:S(2)}) async-start(bf16[4,128,384]{1,2,0:T(8,128)(2,1)} %copy_bitcast_fusion), calls=%async_computation | async-start | bytes 786432 | tf_op jit(solution)/shard_map/all_to_all | solution.py:160
  162.7 7.9 %all-to-all-start.1 = ((bf16[4,128,128]{1,2,0:T(8,128)(2,1)}), bf16[4,128,128]{1,2,0:T(8,128)(2,1)S(1)}, u32[]{:S(2)}, u32[]{:S(2)}) async-start(bf16[4,128,128]{1,2,0:T(8,128)(2,1)} %copy_bitcast_fusion.1), calls=%async_computation.1 | async-start | bytes 262144 | tf_op jit(solution)/shard_map/all_to_all | solution.py:161
  166.0 34.0 %all-gather.14.cloned.1.call-start = ((), (), s32[]{:S(2)}) async-start(), calls=%async_computation.5 | async-start | bytes 2621440 | tf_op jit(solution)/shard_map/all_gather | solution.py:172
  170.1 2.7 copy-start.5
  170.1 2.7 copy-start.14
  170.1 3.0 copy-start.15
  174.1 152.3 %all-gather.16.cloned.1.call-start = ((), (), s32[]{:S(2)}) async-start(), calls=%async_computation.6 | async-start | bytes 9437184 | tf_op jit(solution)/shard_map/all_gather | solution.py:176
  174.7 276.8 %all-gather.18.cloned.1.call-start = ((), (), s32[]{:S(2)}) async-start(), calls=%async_computation.7 | async-start | bytes 9437184 | tf_op jit(solution)/shard_map/all_gather | solution.py:183
  175.3 323.5 %copy-start.16 = (f32[2048]{0:T(1024)S(1)}, f32[2048]{0:T(1024)}, u32[]{:S(2)}) copy-start(f32[2048]{0:T(1024)} %param.41) | copy-start | bytes 24580
  175.3 322.2 %reduce-scatter.2.cloned.1.call-start = ((), (), s32[]{:S(2)}) async-start(), calls=%async_computation.8 | async-start | bytes 2621440 | tf_op jit(solution)/shard_map/reduce_scatter | solution.py:186
Sparse Core Ops, SparseCore 0:
  8.9 49.0 all-gather.9
  59.6 22.5 all-gather.11
  174.3 25.6 all-gather.13
  201.9 124.4 all-gather.15
  328.3 123.1 all-gather.17
  468.1 29.3 reduce-scatter.1
where the time goes:
time: 509 us; the launch traced here: 508 us
  waiting for transfers between devices  313 us (61%)
  blocking collectives  88 us (17%)
  matrix products  31.6 us (6%)
  local copies, waits for them, and re-layouts  26.2 us (5%)
  other arithmetic  26.1 us (5%)
  between operations  15.2 us (3%)
  starting transfers between devices  7.16 us (1%)
    all_gather x1, waiting for transfers between devices, local(): lax.all_gather(up_weight, 'sp', axis=0, tiled=True)  126 us
    all_gather x1, waiting for transfers between devices, local(): lax.all_gather(down_weight, 'sp', axis=1, tiled=True)  125 us
    all_gather x2, blocking collectives, prefix_2(): lax.all_gather(a.astype(kind), axis)  66.6 us
    reduce_scatter x1, waiting for transfers between devices, local(): lax.psum_scatter(partial_terms.astype(jnp.bfloat16), 'tp', scatter_dimens...  29.5 us
    all_gather x1, waiting for transfers between devices, local(): block_rows = lax.all_gather(normed, 'tp', axis=0, tiled=True)  24.6 us
    unnamed x1, blocking collectives  21.4 us
    dot_general x1, matrix products, local(): jnp.dot(hidden, lax.all_gather(down_weight, 'sp', axis=1, tiled=True), pr...  16.5 us
  transfers between devices with their start and end apart: 8, of which 6 were waited for; matrix products, arithmetic and copies ran while one was open for 12% of the time, Pallas kernels for 0%

commit v1 on v0

--- a/solution.py
+++ b/solution.py
@@ -7,6 +7,11 @@
 NARROW_DIM = 64
 SPAN = 128
 epsilon = 1e-06
+
+
+def gather_blocks(value, axis, dim):
+    blocks = lax.all_gather(value, axis)
+    return jnp.concatenate(blocks, axis=dim)
 
 
 def prefix_2(array, axis, join, neutral):
@@ -179,9 +184,7 @@
     )
     hidden = (rectified * rectified).astype(jnp.bfloat16)
     partial_terms = jnp.dot(
-        hidden,
-        lax.all_gather(down_weight, "sp", axis=1, tiled=True),
-        preferred_element_type=jnp.float32,
+        hidden, gather_blocks(down_weight, "sp", 1), preferred_element_type=jnp.float32
     )
     lowered = lax.psum_scatter(
         partial_terms.astype(jnp.bfloat16), "tp", scatter_dimension=0, tiled=True

time: 509 us -> 422 us (0.83)
  waiting for transfers between devices: 313 us -> 220 us
  local copies, waits for them, and re-layouts: 26.2 us -> 33.1 us
  blocking collectives: 88 us -> 94.7 us
  other arithmetic: 26.1 us -> 20 us
    all_gather x1, waiting for transfers between devices: 125 us -> 45.1 us  [gather_blocks(): blocks = lax.all_gather(value, axis)]
    all_gather x1, waiting for transfers between devices: 24.6 us -> 10.6 us  [local(): block_rows = lax.all_gather(normed, 'tp', axis=0, tiled=True)]
    reshape x0 -> x1, local copies, waits for them, and re-layouts: none -> 11.6 us  [gather_blocks(): return jnp.concatenate(blocks, axis=dim)]
  transfers between devices with their start and end apart: 8 -> 8, of which waited for: 6 -> 6; matrix products, arithmetic and copies ran while one was open for 12% -> 15% of each run, Pallas kernels for 0% -> 0%
where the time goes in v1:
time: 422 us; the launch traced here: 420 us
  waiting for transfers between devices  220 us (52%)
  blocking collectives  94.7 us (22%)
  local copies, waits for them, and re-layouts  33.1 us (8%)
  matrix products  29.9 us (7%)
  other arithmetic  20 us (5%)
  between operations  15.4 us (4%)
  starting transfers between devices  7.16 us (2%)
    all_gather x1, waiting for transfers between devices, local(): lax.all_gather(up_weight, 'sp', axis=0, tiled=True)  126 us
    all_gather x2, blocking collectives, prefix_2(): lax.all_gather(a.astype(kind), axis)  71 us
    all_gather x1, waiting for transfers between devices, gather_blocks(): blocks = lax.all_gather(value, axis)  45.1 us
    reduce_scatter x1, waiting for transfers between devices, local(): lax.psum_scatter(partial_terms.astype(jnp.bfloat16), 'tp', scatter_dimens...  29.5 us
    unnamed x1, blocking collectives  23.7 us
    dot_general x1, matrix products, local(): jnp.dot(hidden, gather_blocks(down_weight, 'sp', 1), preferred_element_ty...  16.5 us
    reshape x1, local copies, waits for them, and re-layouts, gather_blocks(): return jnp.concatenate(blocks, axis=dim)  11.6 us
    all_gather x1, waiting for transfers between devices, local(): block_rows = lax.all_gather(normed, 'tp', axis=0, tiled=True)  10.6 us
  transfers between devices with their start and end apart: 8, of which 6 were waited for; matrix products, arithmetic and copies ran while one was open for 15% of the time, Pallas kernels for 0%

profile of v1, /device:TPU:0, one launch (start us, length us, event | category | flops | bytes accessed | tf_op | source)
XLA Modules:
  0.0 420.1 jit_solution(10806266527916559806)
XLA Ops:
  6.5 0.7 all-gather.11.cloned.1.call-update
  7.3 0.7 all-gather.13.cloned.1.call-update
  8.1 0.7 all-gather.19.cloned.1.call-update
  8.8 1.2 copy.119
  11.0 1.0 subtract_convert_fusion
  16.8 23.7 %all-reduce.2 = (bf16[24]{0:T(256)(128)(2,1)}, bf16[16]{0:T(256)(128)(2,1)}) all-reduce(bf16[24]{0:T(256)(128)(2,1)S(1)} %dynamic-update-slice, bf16[16]{0:T(256)(128)(2,1)S(1)} %dynamic-update-slice.1), channel_id=2, replica_groups=mesh['sp'=8,'tp'=4] {'sp'}, use_global_device_ids=true, to_apply=%add | all-reduce | flops 40 | bytes 160
  40.5 0.8 fusion.76
  41.3 1.4 reshape.394
  42.8 0.8 fusion.33
  43.6 3.3 while.42
  43.6 0.7 bitcast_dynamic-update-slice_fusion.8
  44.4 0.7 bitcast_dynamic-update-slice_fusion.8
  45.2 0.7 bitcast_dynamic-update-slice_fusion.8
  46.0 0.7 bitcast_dynamic-update-slice_fusion.8
  47.5 1.0 copy.135
  48.6 1.0 copy.148
  50.4 0.8 fusion.74
  51.9 0.7 fusion.61
  52.9 2.9 while.43
  56.4 1.3 reshape.378
  57.7 1.3 reshape.380
  59.0 1.0 concatenate.34
  60.3 0.7 concatenate.35
  61.0 1.2 copy.121
  62.2 1.1 copy.144
  63.3 1.1 copy.126
  64.4 33.3 %all-gather.3 = bf16[16,64,64]{2,1,0:T(8,128)(2,1)} all-gather(bf16[2,64,64]{2,1,0:T(8,128)(2,1)} %convert_element_type.158), channel_id=5, replica_groups=mesh['sp'=8,'tp'=4] {'sp'}, dimensions={0}, use_global_device_ids=true | all-gather | bytes 147456 | tf_op jit(solution)/shard_map/all_gather | solution.py:20
  98.3 1.3 subtract_exponential_fusion
  99.6 37.7 %all-gather.1 = bf16[24,128,128]{2,1,0:T(8,128)(2,1)} all-gather(bf16[3,128,128]{2,1,0:T(8,128)(2,1)} %convert_element_type.154), channel_id=3, replica_groups=mesh['sp'=8,'tp'=4] {'sp'}, dimensions={0}, use_global_device_ids=true | all-gather | bytes 884736 | tf_op jit(solution)/shard_map/all_gather | solution.py:20
  137.3 2.6 fusion.8
  139.9 3.1 multiply_reduce_fusion.1
  143.1 1.8 copy.145
  144.9 1.2 copy.146
  146.3 0.8 copy_bitcast_fusion
  147.1 3.5 all-to-all-start
  153.1 4.8 %all-to-all-done = bf16[4,128,384]{1,2,0:T(8,128)(2,1)S(1)} async-done(((bf16[4,128,384]{1,2,0:T(8,128)(2,1)}), bf16[4,128,384]{1,2,0:T(8,128)(2,1)S(1)}, u32[]{:S(2)}, u32[]{:S(2)}) %all-to-all-start) | async-done | bytes 393248 | tf_op jit(solution)/shard_map/all_to_all | solution.py:165
  158.0 3.3 all-to-all-start.1
  161.6 3.8 fusion.77
  165.9 2.1 multiply_reduce_fusion
  168.5 1.0 fusion.20
  170.1 45.1 %all-gather.19.cloned.1.call-done = bf16[16384,256]{1,0:T(8,128)(2,1)} async-done(((bf16[2048,256]{1,0:T(8,128)(2,1)}), bf16[16384,256]{1,0:T(8,128)(2,1)}) %all-gather.19.cloned.1.call-update) | async-done | bytes 8388624 | tf_op jit(solution)/shard_map/all_gather | solution.py:13
  215.2 11.6 %copy.160 = bf16[2048,8,256]{0,2,1:T(8,128)(2,1)} copy(bf16[2048,8,256]{2,0,1:T(8,128)(2,1)} %bitcast.172) | data formatting | bytes 16777216 | tf_op jit(solution)/shard_map/reshape | solution.py:14
  226.7 10.6 %all-gather.15.cloned.1.call-done = bf16[512,2048]{1,0:T(8,128)(2,1)} async-done(((bf16[128,2048]{1,0:T(8,128)(2,1)}), bf16[512,2048]{1,0:T(8,128)(2,1)}) %all-gather.15.cloned.1.call-update) | async-done | bytes 2097168 | tf_op jit(solution)/shard_map/all_gather | solution.py:177
  237.4 126.5 %all-gather.17.cloned.1.call-done = bf16[2048,2048]{1,0:T(8,128)(2,1)} async-done(((bf16[256,2048]{1,0:T(8,128)(2,1)}), bf16[2048,2048]{1,0:T(8,128)(2,1)}) %all-gather.17.cloned.1.call-update) | async-done | bytes 8388624 | tf_op jit(solution)/shard_map/all_gather | solution.py:181
  363.8 16.5 %convolution_convert_fusion = bf16[512,2048]{1,0:T(8,128)(2,1)} fusion(bf16[2048,2048]{0,1:T(8,128)(2,1)} %bitcast.173, bf16[512,2048]{1,0:T(8,128)(2,1)} %all-gather.15.cloned.1.call-done, bf16[2048,2048]{1,0:T(8,128)(2,1)} %all-gather.17.cloned.1.call-done), kind=kOutput, calls=%fused_computation.19 | convolution fusion | flops 8594128896 | bytes 20971520 | tf_op jit(solution)/shard_map/dot_general | solution.py:186
  380.4 29.5 %reduce-scatter.2.cloned.1.call-done = bf16[128,2048]{1,0:T(8,128)(2,1)} async-done(((bf16[512,2048]{1,0:T(8,128)(2,1)}), bf16[128,2048]{1,0:T(8,128)(2,1)}) %reduce-scatter.2.cloned.1.call-update) | async-done | bytes 524304 | tf_op jit(solution)/shard_map/reduce_scatter | solution.py:189
  409.9 1.2 fusion.16
  411.1 2.1 fusion.21
  (144 shorter events, 16.2 us)
Async XLA Ops:
  6.5 3.6 copy-start.6
  6.5 155.0 %all-gather.11.cloned.1.call-start = ((), (), s32[]{:S(2)}) async-start(), calls=%async_computation.3 | async-start | bytes 7864320 | tf_op jit(solution)/shard_map/all_gather | solution.py:169
  7.3 158.6 %all-gather.13.cloned.1.call-start = ((), (), s32[]{:S(2)}) async-start(), calls=%async_computation.4 | async-start | bytes 2621440 | tf_op jit(solution)/shard_map/all_gather | solution.py:170
  8.0 207.2 %all-gather.19.cloned.1.call-start = ((), (), s32[]{:S(2)}) async-start(), calls=%async_computation.8 | async-start | bytes 9437184 | tf_op jit(solution)/shard_map/all_gather | solution.py:13
  10.3 2.6 copy-start.19
  10.4 2.9 copy-start.20
  10.9 2.8 copy-start.21
  13.3 28.0 %copy-start = (f32[4,128,3]{2,1,0:T(8,128)}, f32[4,128,3]{2,1,0:T(8,128)S(1)}, u32[]{:S(2)}) copy-start(f32[4,128,3]{2,1,0:T(8,128)S(1)} %reduce_window_sum.44) | copy-start | bytes 18436
  43.6 7.7 %copy-start.10 = (bf16[512,128]{1,0:T(8,128)(2,1)S(1)}, bf16[512,128]{1,0:T(8,128)(2,1)}, u32[]{:S(2)}) copy-start(bf16[512,128]{1,0:T(8,128)(2,1)} %param.30) | copy-start | bytes 393220
  46.8 13.4 %copy-start.13 = (f32[4,3]{1,0:T(4,128)}, f32[4,3]{1,0:T(4,128)S(1)}, u32[]{:S(2)}) copy-start(f32[4,3]{1,0:T(4,128)S(1)} %get-tuple-element.474) | copy-start | bytes 148
  47.5 12.8 %copy-start.2 = (bf16[512,3,64]{0,2,1:T(8,128)(2,1)S(1)}, bf16[512,3,64]{0,2,1:T(8,128)(2,1)}, u32[]{:S(2)}) copy-start(bf16[512,3,64]{0,2,1:T(8,128)(2,1)} %get-tuple-element.234) | copy-start | bytes 589828
  49.7 0.6 copy-start.14
  52.7 6.3 %copy-start.3 = (f32[4,128,2,64]{1,3,2,0:T(8,128)}, f32[4,128,2,64]{1,3,2,0:T(8,128)S(1)}, u32[]{:S(2)}) copy-start(f32[4,128,2,64]{1,3,2,0:T(8,128)S(1)} %bitcast_dynamic-update-slice_fusion.2) | copy-start | bytes 786436
  139.9 11.2 %copy-start.8 = (bf16[2,4,4,8,128]{4,3,2,1,0:T(8,128)(2,1)S(1)}, bf16[2,4,4,8,128]{4,3,2,1,0:T(8,128)(2,1)}, u32[]{:S(2)}) copy-start(bf16[2,4,4,8,128]{4,3,2,1,0:T(8,128)(2,1)} %get-tuple-element.238) | copy-start | bytes 196612
  143.0 7.6 %copy-start.15 = (f32[4,1,2]{0,2,1:T(2,128)S(1)}, f32[4,1,2]{0,2,1:T(2,128)}, u32[]{:S(2)}) copy-start(f32[4,1,2]{0,2,1:T(2,128)} %copy-done.14) | copy-start | bytes 100
  143.0 7.8 %copy-start.1 = (f32[4,128,2]{2,1,0:T(8,128)S(1)}, f32[4,128,2]{2,1,0:T(8,128)}, u32[]{:S(2)}) copy-start(f32[4,128,2]{2,1,0:T(8,128)} %get-tuple-element.241) | copy-start | bytes 12292
  143.0 8.1 %copy-start.7 = (bf16[2,4,4,8,128]{4,3,2,1,0:T(8,128)(2,1)S(1)}, bf16[2,4,4,8,128]{4,3,2,1,0:T(8,128)(2,1)}, u32[]{:S(2)}) copy-start(bf16[2,4,4,8,128]{4,3,2,1,0:T(8,128)(2,1)} %get-tuple-element.237) | copy-start | bytes 196612
  143.0 8.2 %copy-start.9 = (f32[4,2,64,64]{3,2,1,0:T(8,128)S(1)}, f32[4,2,64,64]{3,2,1,0:T(8,128)}, u32[]{:S(2)}) copy-start(f32[4,2,64,64]{3,2,1,0:T(8,128)} %get-tuple-element.136) | copy-start | bytes 393220
  143.0 8.5 %copy-start.4 = (f32[4,128,2,64]{1,3,2,0:T(8,128)S(1)}, f32[4,128,2,64]{1,3,2,0:T(8,128)}, u32[]{:S(2)}) copy-start(f32[4,128,2,64]{1,3,2,0:T(8,128)} %copy-done.3) | copy-start | bytes 786436
  143.1 8.5 %copy-start.12 = (pred[128,128]{1,0:T(8,128)(4,1)S(1)}, pred[128,128]{1,0:T(8,128)(4,1)}, u32[]{:S(2)}) copy-start(pred[128,128]{1,0:T(8,128)(4,1)} %iota_compare_fusion) | copy-start | bytes 49156
  143.1 9.2 %copy-start.11 = (bf16[512,128]{1,0:T(8,128)(2,1)S(1)}, bf16[512,128]{1,0:T(8,128)(2,1)}, u32[]{:S(2)}) copy-start(bf16[512,128]{1,0:T(8,128)(2,1)} %param.31) | copy-start | bytes 393220
  147.1 10.8 %all-to-all-start = ((bf16[4,128,384]{1,2,0:T(8,128)(2,1)}), bf16[4,128,384]{1,2,0:T(8,128)(2,1)S(1)}, u32[]{:S(2)}, u32[]{:S(2)}) async-start(bf16[4,128,384]{1,2,0:T(8,128)(2,1)} %copy_bitcast_fusion), calls=%async_computation | async-start | bytes 786432 | tf_op jit(solution)/shard_map/all_to_all | solution.py:165
  158.0 7.9 %all-to-all-start.1 = ((bf16[4,128,128]{1,2,0:T(8,128)(2,1)}), bf16[4,128,128]{1,2,0:T(8,128)(2,1)S(1)}, u32[]{:S(2)}, u32[]{:S(2)}) async-start(bf16[4,128,128]{1,2,0:T(8,128)(2,1)} %copy_bitcast_fusion.1), calls=%async_computation.1 | async-start | bytes 262144 | tf_op jit(solution)/shard_map/all_to_all | solution.py:166
  161.3 76.0 %all-gather.15.cloned.1.call-start = ((), (), s32[]{:S(2)}) async-start(), calls=%async_computation.5 | async-start | bytes 2621440 | tf_op jit(solution)/shard_map/all_gather | solution.py:177
  165.4 2.7 copy-start.5
  165.4 2.7 copy-start.16
  165.4 3.0 copy-start.17
  169.5 194.4 %all-gather.17.cloned.1.call-start = ((), (), s32[]{:S(2)}) async-start(), calls=%async_computation.6 | async-start | bytes 9437184 | tf_op jit(solution)/shard_map/all_gather | solution.py:181
  170.1 239.9 %reduce-scatter.2.cloned.1.call-start = ((), (), s32[]{:S(2)}) async-start(), calls=%async_computation.7 | async-start | bytes 2621440 | tf_op jit(solution)/shard_map/reduce_scatter | solution.py:189
  363.8 47.3 %copy-start.18 = (f32[2048]{0:T(1024)S(1)}, f32[2048]{0:T(1024)}, u32[]{:S(2)}) copy-start(f32[2048]{0:T(1024)} %param.41) | copy-start | bytes 24580
Sparse Core Ops, SparseCore 0:
  8.9 49.0 all-gather.10
  59.6 22.5 all-gather.12
  84.3 130.8 all-gather.18
  216.6 20.7 all-gather.14
  239.3 124.4 all-gather.16
  380.5 29.3 reduce-scatter.1
